TPU v7x, 256 devices: a whole 4x4x8 slice. The times are simulated.
256 devices in a mesh: sp: 32 (over z, y), dp: 8 (over x, core).
Axes of the slice: x: 4, y: 4, z: 8, core: 2. Of those that a mesh axis runs over, the one named last changes fastest.
Arguments:
- queries: bfloat16 [32768, 6144], P(('dp', 'sp')), may hold values from -360 to 360
- latent: bfloat16 [32768, 1024], P(('dp', 'sp')), may hold values from -6 to 6
- rope_key: bfloat16 [32768, 64], P(('dp', 'sp')), may hold values from -6 to 6
- latent_gain: float32 [1024], replicated, may hold values from 0.1 to 1.9
- kv_weight: bfloat16 [1024, 8192], P(None, 'dp'), may hold values from -0.1875 to 0.1875
- gate: bfloat16 [32768, 4096], P(('dp', 'sp')), may hold values from -6 to 6
- out_gain: float32 [4096], replicated, may hold values from 0.1 to 1.9
Outputs:
- attended: bfloat16 [32768, 4096], P(('dp', 'sp'))
All inputs are finite; a program needn't handle non-finite values.
Results may differ from a plain program's by a relative error of at most 0.007.
Values may be sent and summed in bfloat16 or wider, within the bound.
A program may use at most 128 MiB of HBM per device.

v0:
```python
import functools

import jax
import jax.numpy as jnp
import numpy as np
from jax import lax
from jax.experimental import pallas as pl
from jax.experimental.pallas import tpu as pltpu
from jax.sharding import PartitionSpec as P

HEADS = 32
NOPE = 128
ROPE = 64
VDIM = 128
QDIM = NOPE + ROPE
PAIR = 2 * QDIM
KDIM = 256

EPS = 1e-06
THETA = 10000.0
LOG2E = 1.4426950408889634

MESH = pl.DeviceIdType.MESH
DN_T = (((1,), (1,)), ((), ()))


def turn(x, cosine, sine, mask):
    partner = jnp.where(mask, pltpu.roll(x, 96, 1), pltpu.roll(x, 32, 1))
    return x * cosine + partner * sine


def kernel(
    n_s, n_d,
    q_ref, lat_ref, rk_ref, lgain_ref, w_ref, gate_ref, ogain_ref, ta_ref, tb_ref,
    out_ref,
    w_v, gate_v, latb, rkb, qb, kbuf, vbuf, rq, ob, orecv,
    w_sem, gate_sem, lat_send, lat_recv, rk_send, rk_recv, relay_lat, relay_rk,
    q_send, q_recv, o_send, o_recv,
):
    s, d = lax.axis_index("sp"), lax.axis_index("dp")
    rows = lat_ref.shape[0]
    heads = HEADS // n_d
    pairs = heads // 2
    groups = n_s // n_d
    half = n_d // 2
    zh, m = s // n_d, s % n_d
    seq = 2 * ((m % half - m // half + half) % half) + m // half
    home = (d % 2) * half + (d // 2 + d % 2) % half
    core = d % 2
    partner = d + 1 - 2 * core

    def send(src, dst, ssem, rsem, ts, td):
        same = (ts == s) & (td == d)

        @pl.when(jnp.logical_not(same))
        def _():
            pltpu.make_async_remote_copy(
                src, dst, ssem, rsem, device_id={"sp": ts, "dp": td}, device_id_type=MESH
            ).start()

        @pl.when(same)
        def _():
            pltpu.make_async_copy(src, dst, rsem).start()

    def sent(src, dst, ssem, rsem, ts, td):
        same = (ts == s) & (td == d)

        @pl.when(jnp.logical_not(same))
        def _():
            pltpu.make_async_remote_copy(
                src, dst, ssem, rsem, device_id={"sp": ts, "dp": td}, device_id_type=MESH
            ).wait_send()

    def arrived(dst, rsem):
        pltpu.make_async_copy(dst, dst, rsem).wait()

    latent_sends = []
    for k in range(groups):
        for pair in range(n_d // 2):
            i = k * (n_d // 2) + pair
            to = (k * n_d + home, 2 * pair + s % 2)
            latent_sends.append((lat_ref, latb.at[s], lat_send.at[i], lat_recv.at[s], *to))
            latent_sends.append((rk_ref, rkb.at[s], rk_send.at[i], rk_recv.at[s], *to))
    query_sends = [
        (
            q_ref.at[:, pl.ds((t * pairs + p) * PAIR, PAIR)], qb.at[m, p],
            q_send.at[t, p], q_recv.at[m, p], zh * n_d + home, jnp.int32(t),
        )
        for p in range(pairs)
        for t in range(n_d)
    ]
    w_copy = pltpu.make_async_copy(w_ref, w_v, w_sem)
    gate_copy = pltpu.make_async_copy(gate_ref, gate_v, gate_sem)

    for args in latent_sends + query_sends:
        send(*args)
    w_copy.start()
    gate_copy.start()
    w_copy.wait()

    lane = lax.broadcasted_iota(jnp.int32, (rows, 128), 1)
    low = lane < 64
    mask = (lane % 64) < 32
    sign = jnp.where(mask, -1.0, 1.0).astype(jnp.float32)

    def tables(block):
        ca, sa = ta_ref[0], ta_ref[1]
        cb, sb = tb_ref[0, block], tb_ref[1, block]
        return ca * cb - sa * sb, (sa * cb + ca * sb) * sign

    def nearest(i):
        if n_s & (n_s - 1):
            return (s + i) % n_s
        out, bit = 0, 1
        while bit < n_s:
            out = out + bit * ((s // bit + i // bit) % 2)
            bit *= 2
        return out

    def key_step(i, carry):
        slot = nearest(i)
        at = pl.ds(pl.multiple_of(slot * rows, rows), rows)
        arrived(latb.at[slot], lat_recv.at[slot])
        arrived(rkb.at[slot], rk_recv.at[slot])

        @pl.when(slot % 2 == core)
        def _():
            for buf, ssem, rsem in ((latb, relay_lat, lat_recv), (rkb, relay_rk, rk_recv)):
                pltpu.make_async_remote_copy(
                    buf.at[slot], buf.at[slot], ssem.at[slot // 2], rsem.at[slot],
                    device_id={"sp": s, "dp": partner}, device_id_type=MESH,
                ).start()

        wide = latb[slot].astype(jnp.float32)
        scale = lax.rsqrt(jnp.mean(wide * wide, axis=-1, keepdims=True) + EPS)
        normed = (wide * scale * lgain_ref[...]).astype(jnp.bfloat16)
        cosine, sine = tables(slot)
        raw = rkb[slot].astype(jnp.float32).T
        rot = turn(jnp.concatenate([raw, jnp.zeros_like(raw)], axis=1), cosine, sine, mask)
        rot_high = pltpu.roll(rot, 64, 1)
        for h in range(heads):
            both = jnp.dot(
                normed, w_v[:, h * 256 : (h + 1) * 256], preferred_element_type=jnp.float32
            )
            plain = both[:, :NOPE]
            if h % 2 == 0:
                first, second = plain, rot
            else:
                moved = pltpu.roll(plain, 64, 1)
                first = jnp.where(low, 0.0, moved)
                second = jnp.where(low, moved, rot_high)
            kbuf[h, at, :128] = first.astype(jnp.bfloat16)
            kbuf[h, at, 128:] = second.astype(jnp.bfloat16)
            vbuf[h, at, :VDIM] = both[:, NOPE:].astype(jnp.bfloat16)
            vbuf[h, at, VDIM:] = jnp.ones((rows, 128), jnp.bfloat16)
        return carry

    lax.fori_loop(0, n_s, key_step, 0)

    factor = LOG2E * QDIM ** -0.5

    def output_send(j, p):
        return (ob.at[j, p], orecv.at[d, p], o_send.at[j, p], o_recv.at[d, p], zh * n_d + j, seq)

    def query_step(i, carry):
        r, p = (i // pairs + m // 2) % half, i % pairs
        for part in range(2):
            slot = 2 * r + part
            arrived(qb.at[slot, p], q_recv.at[slot, p])
            cosine, sine = tables(zh * n_d + slot)
            cosine_high, sine_high = pltpu.roll(cosine, 64, 1), pltpu.roll(sine, 64, 1)
            here = slice(part * rows, (part + 1) * rows)
            rq[here, :128] = qb[slot, p, :, :128]
            x = qb[slot, p, :, 128:256].astype(jnp.float32)
            rq[here, 128:256] = turn(x, cosine, sine, mask).astype(jnp.bfloat16)
            x = qb[slot, p, :, 256:].astype(jnp.float32)
            rq[here, 256:] = turn(x, cosine_high, sine_high, mask).astype(jnp.bfloat16)
        for odd in range(2):
            h = 2 * p + odd
            scores = lax.dot_general(
                rq[:, odd * 128 : odd * 128 + KDIM], kbuf[h], DN_T, preferred_element_type=jnp.float32
            )
            top = jnp.max(scores, axis=-1, keepdims=True)
            raised = jnp.exp2((scores - top) * factor).astype(jnp.bfloat16)
            total = jnp.dot(raised, vbuf[h], preferred_element_type=jnp.float32)
            result = (total[:, :VDIM] / total[:, VDIM:]).astype(jnp.bfloat16)
            at = slice(odd * VDIM, (odd + 1) * VDIM)
            ob[2 * r, p, :, at] = result[:rows]
            ob[2 * r + 1, p, :, at] = result[rows:]
        send(*output_send(2 * r, p))
        send(*output_send(2 * r + 1, p))
        return carry

    lax.fori_loop(0, half * pairs, query_step, 0)

    gate_copy.wait()
    def gated_piece(t, p):
        c = (t * pairs + p) * 2 * VDIM
        g = gate_v[:, c : c + 2 * VDIM].astype(jnp.float32)
        return slice(c, c + 2 * VDIM), orecv[t, p].astype(jnp.float32) * (g / (1.0 + jnp.exp(-g)))

    square = jnp.zeros((rows, 1), jnp.float32)
    for p in range(pairs):
        for t in range(n_d):
            arrived(orecv.at[t, p], o_recv.at[t, p])
            _, gated = gated_piece(t, p)
            square = square + jnp.sum(gated * gated, axis=-1, keepdims=True)
    scale = lax.rsqrt(square / (HEADS * VDIM) + EPS)
    for t in range(n_d):
        for p in range(pairs):
            cols, gated = gated_piece(t, p)
            out_ref[:, cols] = (gated * scale * ogain_ref[:, cols]).astype(jnp.bfloat16)

    for args in latent_sends + query_sends:
        sent(*args)
    for part in range(n_s // 2):
        slot = 2 * part + core
        for buf, ssem, rsem in ((latb, relay_lat, lat_recv), (rkb, relay_rk, rk_recv)):
            pltpu.make_async_remote_copy(
                buf.at[slot], buf.at[slot], ssem.at[part], rsem.at[slot],
                device_id={"sp": s, "dp": partner}, device_id_type=MESH,
            ).wait_send()

    def output_sent(i, carry):
        sent(*output_send(i // pairs, i % pairs))
        return carry

    lax.fori_loop(0, n_d * pairs, output_sent, 0)


def angle_tables(rows, n_s):
    half = ROPE // 2
    inverse = np.zeros(128)
    inverse[:ROPE] = np.tile(THETA ** (-np.arange(half) / half), 2)
    inner = np.arange(rows)[:, None] * inverse[None, :]
    outer = (np.arange(n_s) * rows)[:, None] * inverse[None, :]
    inner = np.stack([np.cos(inner), np.sin(inner)]).astype(np.float32)
    outer = np.stack([np.cos(outer), np.sin(outer)]).astype(np.float32)
    return jnp.asarray(inner), jnp.asarray(outer[:, :, None, :])


def per_device(n_s, n_d, queries, latent, rope_key, latent_gain, kv_weight, gate, out_gain):
    rows, rank = latent.shape
    heads = HEADS // n_d
    pairs = heads // 2
    seq = rows * n_s
    inner, outer = angle_tables(rows, n_s)
    bf = jnp.bfloat16
    dma = pltpu.SemaphoreType.DMA
    vmem = pl.BlockSpec(memory_space=pltpu.VMEM)
    hbm = pl.BlockSpec(memory_space=pl.ANY)
    pieces = n_s // 2
    return pl.pallas_call(
        functools.partial(kernel, n_s, n_d),
        out_shape=jax.ShapeDtypeStruct(gate.shape, bf),
        in_specs=[hbm, vmem, vmem, vmem, hbm, hbm, vmem, vmem, vmem],
        out_specs=vmem,
        scratch_shapes=[
            pltpu.VMEM(kv_weight.shape, bf),
            pltpu.VMEM(gate.shape, bf),
            pltpu.VMEM((n_s, rows, rank), bf),
            pltpu.VMEM((n_s, ROPE, rows), bf),
            pltpu.VMEM((n_d, pairs, rows, PAIR), bf),
            pltpu.VMEM((heads, seq, KDIM), bf),
            pltpu.VMEM((heads, seq, 2 * VDIM), bf),
            pltpu.VMEM((2 * rows, PAIR), bf),
            pltpu.VMEM((n_d, pairs, rows, 2 * VDIM), bf),
            pltpu.VMEM((n_d, pairs, rows, 2 * VDIM), bf),
            dma, dma,
            dma((pieces,)), dma((n_s,)), dma((pieces,)), dma((n_s,)),
            dma((pieces,)), dma((pieces,)),
            *[dma((n_d, pairs))] * 4,
        ],
        compiler_params=pltpu.CompilerParams(
            has_side_effects=True, vmem_limit_bytes=60 * 1024 * 1024
        ),
        name="latent_attention",
    )(
        queries, latent, rope_key.T, latent_gain[None, :], kv_weight, gate, out_gain[None, :],
        inner, outer,
    )


def solution(mesh):
    return jax.shard_map(
        functools.partial(per_device, mesh.shape["sp"], mesh.shape["dp"]),
        mesh=mesh,
        in_specs=(
            P(("dp", "sp"), None),
            P(("dp", "sp"), None),
            P(("dp", "sp"), None),
            P(),
            P(None, "dp"),
            P(("dp", "sp"), None),
            P(),
        ),
        out_specs=P(("dp", "sp"), None),
        check_vma=False,
    )
```

profile of v0, /device:TPU:248, one launch (start us, length us, event | category | flops | bytes accessed | tf_op | source)
XLA Modules:
  0.0 231.2 jit_solution(17995902535459922168)
XLA Ops:
  0.0 228.9 %latent_attention.1 = bf16[128,4096]{1,0:T(8,128)(2,1)} custom-call(bf16[128,6144]{1,0:T(8,128)(2,1)} %q_ref.1, bf16[128,1024]{1,0:T(8,128)(2,1)} %lat_ref.1, bf16[64,128]{1,0:T(8,128)(2,1)} %bitcast.3, f32[1,1024]{1,0:T(1,128)} %bitcast.5, bf16[1024,1024]{1,0:T(8,128)(2,1)} %w_ref.1, bf16[128,4096]{1,0:T(8,128)(2,1)} %gate_ref.1, f32[1,4096]{1,0:T(1,128)} %bitcast.4, ...), custom_call_target="tpu_custom_call" | custom-call | tf_op jit(solution)/shard_map/latent_attention/pallas_call | solution.py:253
  228.9 2.3 copy.11
where the time goes:
time: 231 us
  Pallas kernels  229 us (99%)
    pallas_call x1, Pallas kernels, per_device(): pl.pallas_call(functools.partial(kernel, n_s, n_d), out_shape=jax.ShapeDt...  229 us

commit v1 on v0

v1 whole, which is shorter than its diff:
```python
import functools

import jax
import jax.numpy as jnp
import numpy as np
from jax import lax
from jax.experimental import pallas as pl
from jax.experimental.pallas import tpu as pltpu
from jax.sharding import PartitionSpec as P

HEADS = 32
NOPE = 128
ROPE = 64
VDIM = 128
QDIM = NOPE + ROPE
PAIR = 2 * QDIM
KDIM = 256
CHUNK = 1024

EPS = 1e-06
THETA = 10000.0
LOG2E = 1.4426950408889634

MESH = pl.DeviceIdType.MESH
DN_T = (((1,), (1,)), ((), ()))

ORDER = (
    (0, 0), (1, 0), (3, 0), (0, 3), (0, 1), (2, 0), (1, 3), (1, 1),
    (3, 1), (3, 3), (0, 2), (2, 1), (2, 3), (1, 2), (3, 2), (2, 2),
)
QUERIES_AT = 11


def turn(x, cosine, sine, mask):
    partner = jnp.where(mask, pltpu.roll(x, 96, 1), pltpu.roll(x, 32, 1))
    return x * cosine + partner * sine


def kernel(
    q_ref, lat_ref, rk_ref, lgain_ref, w_ref, gate_ref, ogain_ref, ta_ref, tb_ref, ka_ref, kb_ref,
    out_ref,
    w_v, q_v, gate_v, silu_v, own_lat, own_rk, latb, rkb, qb, kbuf, vbuf, ob, orecv,
    w_sem, q_sem, gate_sem, own_send, lat_send, lat_recv, rk_send, rk_recv,
    q_send, q_recv, o_send, o_recv,
):
    s, d = lax.axis_index("sp"), lax.axis_index("dp")
    rows = lat_ref.shape[0]
    z, y = s // 4, s % 4
    x, c = d // 2, d % 2
    k, par = z // 2, z % 2
    m = par * 4 + y
    seq = 2 * ((y + 4 - par) % 4) + par
    home = c * 4 + (x + c) % 4
    pairs = 2

    def send(src, dst, ssem, rsem, ts, td):
        same = (ts == s) & (td == d)

        @pl.when(jnp.logical_not(same))
        def _():
            pltpu.make_async_remote_copy(
                src, dst, ssem, rsem, device_id={"sp": ts, "dp": td}, device_id_type=MESH
            ).start()

        @pl.when(same)
        def _():
            pltpu.make_async_copy(src, dst, rsem).start()

    def sent(src, dst, ssem, rsem, ts, td):
        same = (ts == s) & (td == d)

        @pl.when(jnp.logical_not(same))
        def _():
            pltpu.make_async_remote_copy(
                src, dst, ssem, rsem, device_id={"sp": ts, "dp": td}, device_id_type=MESH
            ).wait_send()

    def arrived(dst, rsem):
        pltpu.make_async_copy(dst, dst, rsem).wait()

    w_copy = pltpu.make_async_copy(w_ref, w_v, w_sem)
    q_copy = pltpu.make_async_copy(q_ref, q_v, q_sem)
    gate_copy = pltpu.make_async_copy(gate_ref, gate_v, gate_sem)
    q_copy.start()
    w_copy.start()
    gate_copy.start()

    wide = lat_ref[...].astype(jnp.float32)
    scale = lax.rsqrt(jnp.mean(wide * wide, axis=-1, keepdims=True) + EPS)
    own_lat[...] = (wide * scale * lgain_ref[...]).astype(jnp.bfloat16)
    half = ROPE // 2
    kca, ksa, kcb, ksb = ka_ref[0], ka_ref[1], kb_ref[0, s], kb_ref[1, s]
    kc, ks = kca * kcb - ksa * ksb, ksa * kcb + kca * ksb
    raw = rk_ref[...].astype(jnp.float32)
    u1, u2 = raw[:half], raw[half:]
    own_rk[:half] = (u1 * kc - u2 * ks).astype(jnp.bfloat16)
    own_rk[half:] = (u2 * kc + u1 * ks).astype(jnp.bfloat16)

    ones = jnp.ones((rows, 128), jnp.bfloat16)

    def ones_step(i, carry):
        at = pl.ds(pl.multiple_of(i * rows, rows), rows)
        for h in range(4):
            vbuf[h, at, VDIM:] = ones
        return carry

    lax.fori_loop(0, vbuf.shape[1] // rows, ones_step, 0)

    first_block = k * 4 + y
    first_to = ((2 * k + c) * 4 + (x + c) % 4, 2 * y + par)
    own_sends = [
        (own_lat, latb.at[first_block, par], own_send.at[0], lat_recv.at[first_block, par], *first_to),
        (own_rk, rkb.at[first_block, par], own_send.at[1], rk_recv.at[first_block, par], *first_to),
    ]
    for args in own_sends:
        send(*args)

    lane = lax.broadcasted_iota(jnp.int32, (rows, 128), 1)
    mask = (lane % 64) < 32
    sign = jnp.where(mask, -1.0, 1.0).astype(jnp.float32)
    ca, sa, cb, sb = ta_ref[0], ta_ref[1], tb_ref[0, s], tb_ref[1, s]
    cosine, sine = ca * cb - sa * sb, (sa * cb + ca * sb) * sign
    cosine_high, sine_high = pltpu.roll(cosine, 64, 1), pltpu.roll(sine, 64, 1)
    q_copy.wait()
    for i in range(HEADS // 2):
        at = slice(i * PAIR + 128, i * PAIR + 256)
        q_v[:, at] = turn(q_v[:, at].astype(jnp.float32), cosine, sine, mask).astype(jnp.bfloat16)
        at = slice(i * PAIR + 256, i * PAIR + 384)
        q_v[:, at] = turn(
            q_v[:, at].astype(jnp.float32), cosine_high, sine_high, mask
        ).astype(jnp.bfloat16)
    query_sends = [
        (
            q_v.at[:, pl.ds((t * pairs + p) * PAIR, PAIR)], qb.at[m, p],
            q_send.at[t, p], q_recv.at[m, p], k * 8 + home, jnp.int32(t),
        )
        for p in range(pairs)
        for t in range(8)
    ]
    gate_copy.wait()
    for i in range(16):
        at = slice(i * 256, (i + 1) * 256)
        g = gate_v[:, at].astype(jnp.float32)
        silu_v[i] = g / (1.0 + jnp.exp(-g))
    w_copy.wait()

    low = lax.broadcasted_iota(jnp.int32, (2 * rows, 128), 1) < 64

    def place(i):
        dk, dx = jnp.int32(0), jnp.int32(0)
        for n, (a, b) in enumerate(ORDER):
            dk = jnp.where(i == n, a, dk)
            dx = jnp.where(i == n, b, dx)
        return dk, dx, ((k + dk) % 4) * 4 + (x + dx) % 4

    def forwards(i, act):
        dk, dx, block = place(i)
        own = dx == 0
        ways = (
            (own | ((dx == 3) & (dk < 2)), s, 2 * ((x + 1) % 4) + c),
            (own | ((dx == 1) & (dk >= 2)), s, 2 * ((x + 3) % 4) + c),
            (own & ((dk == 0) | ((dk == 3) & (c == 0))), ((z + 2) % 8) * 4 + y, d),
            (own & ((dk == 0) | ((dk == 1) & (c == 1))), ((z + 6) % 8) * 4 + y, d),
            (None, s, 2 * x + 1 - c),
        )
        for n, (when, ts, td) in enumerate(ways):
            def go(n=n, ts=ts, td=td):
                for buf, ssem, rsem in ((latb, lat_send, lat_recv), (rkb, rk_send, rk_recv)):
                    act(pltpu.make_async_remote_copy(
                        buf.at[block, c], buf.at[block, c], ssem.at[i, n], rsem.at[block, c],
                        device_id={"sp": ts, "dp": td}, device_id_type=MESH,
                    ))

            if when is None:
                go()
            else:
                pl.when(when)(go)

    def key_step(i, carry):
        _, _, block = place(i)
        arrived(latb.at[block, c], lat_recv.at[block, c])
        arrived(rkb.at[block, c], rk_recv.at[block, c])
        forwards(i, lambda copy: copy.start())

        @pl.when(i == QUERIES_AT)
        def _():
            for args in query_sends:
                send(*args)

        arrived(latb.at[block, 1 - c], lat_recv.at[block, 1 - c])
        arrived(rkb.at[block, 1 - c], rk_recv.at[block, 1 - c])
        at = pl.ds(pl.multiple_of(i * 2 * rows, 2 * rows), 2 * rows)
        normed = latb[block].reshape(2 * rows, lat_ref.shape[1])
        both_rk = jnp.concatenate([rkb[block, 0], rkb[block, 1]], axis=1).astype(jnp.float32)
        rot = jnp.concatenate([both_rk, jnp.zeros_like(both_rk)], axis=0).T
        rot_high = pltpu.roll(rot, 64, 1)
        for h in range(4):
            both = jnp.dot(
                normed, w_v[:, h * 256 : (h + 1) * 256], preferred_element_type=jnp.float32
            )
            plain = both[:, :NOPE]
            if h % 2 == 0:
                first, second = plain, rot
            else:
                moved = pltpu.roll(plain, 64, 1)
                first = jnp.where(low, 0.0, moved)
                second = jnp.where(low, moved, rot_high)
            kbuf[h, at, :128] = first.astype(jnp.bfloat16)
            kbuf[h, at, 128:] = second.astype(jnp.bfloat16)
            vbuf[h, at, :VDIM] = both[:, NOPE:].astype(jnp.bfloat16)
        return carry

    lax.fori_loop(0, 16, key_step, 0)

    factor = LOG2E * QDIM ** -0.5
    n_chunks = kbuf.shape[1] // CHUNK

    def output_send(j, p):
        return (ob.at[j, p], orecv.at[d, p], o_send.at[j, p], o_recv.at[d, p], k * 8 + j, seq)

    def query_step(i, carry):
        r, p = (i // pairs + m // 2) % 4, i % pairs
        for part in range(2):
            arrived(qb.at[2 * r + part, p], q_recv.at[2 * r + part, p])
        for odd in range(2):
            h = 2 * p + odd
            at = slice(odd * 128, odd * 128 + KDIM)
            q = jnp.concatenate([qb[2 * r, p, :, at], qb[2 * r + 1, p, :, at]], axis=0)

            def score(j):
                return lax.dot_general(
                    q, kbuf[h, j * CHUNK : (j + 1) * CHUNK], DN_T, preferred_element_type=jnp.float32
                )

            following = score(0)
            for j in range(n_chunks):
                scores = following
                if j + 1 < n_chunks:
                    following = score(j + 1)
                top = jnp.max(scores, axis=-1, keepdims=True)
                if j:
                    top = jnp.maximum(top, before)
                raised = jnp.exp2((scores - top) * factor).astype(jnp.bfloat16)
                part_total = jnp.dot(
                    raised, vbuf[h, j * CHUNK : (j + 1) * CHUNK], preferred_element_type=jnp.float32
                )
                total = total * jnp.exp2((before - top) * factor) + part_total if j else part_total
                before = top
            result = (total[:, :VDIM] / total[:, VDIM:]).astype(jnp.bfloat16)
            at = slice(odd * VDIM, (odd + 1) * VDIM)
            ob[2 * r, p, :, at] = result[:rows]
            ob[2 * r + 1, p, :, at] = result[rows:]
        send(*output_send(2 * r, p))
        send(*output_send(2 * r + 1, p))
        return carry

    lax.fori_loop(0, 4 * pairs, query_step, 0)

    square = jnp.zeros((rows, 1), jnp.float32)
    for p in range(pairs):
        for t in range(8):
            arrived(orecv.at[t, p], o_recv.at[t, p])
            gated = orecv[t, p].astype(jnp.float32) * silu_v[t * pairs + p]
            silu_v[t * pairs + p] = gated
            square = square + jnp.sum(gated * gated, axis=-1, keepdims=True)
    scale = lax.rsqrt(square / (HEADS * VDIM) + EPS)
    for i in range(16):
        cols = slice(i * 256, (i + 1) * 256)
        out_ref[:, cols] = (silu_v[i] * scale * ogain_ref[:, cols]).astype(jnp.bfloat16)

    for args in own_sends + query_sends:
        sent(*args)

    def forwards_sent(i, carry):
        forwards(i, lambda copy: copy.wait_send())
        return carry

    lax.fori_loop(0, 16, forwards_sent, 0)

    def output_sent(i, carry):
        sent(*output_send(i // pairs, i % pairs))
        return carry

    lax.fori_loop(0, 8 * pairs, output_sent, 0)


def angle_tables(rows, n_s):
    half = ROPE // 2
    base = THETA ** (-np.arange(half) / half)
    inverse = np.zeros(128)
    inverse[:ROPE] = np.tile(base, 2)

    def both(angles):
        return np.stack([np.cos(angles), np.sin(angles)]).astype(np.float32)

    inner, outer = np.arange(rows), np.arange(n_s) * rows
    return (
        both(inner[:, None] * inverse[None, :]),
        both(outer[:, None] * inverse[None, :])[:, :, None, :],
        both(base[:, None] * inner[None, :]),
        both(outer[:, None] * base[None, :])[:, :, :, None],
    )


def per_device(n_s, n_d, queries, latent, rope_key, latent_gain, kv_weight, gate, out_gain):
    rows, rank = latent.shape
    heads = HEADS // n_d
    pairs = heads // 2
    seq = rows * n_s
    tables = [jnp.asarray(t) for t in angle_tables(rows, n_s)]
    bf = jnp.bfloat16
    dma = pltpu.SemaphoreType.DMA
    vmem = pl.BlockSpec(memory_space=pltpu.VMEM)
    hbm = pl.BlockSpec(memory_space=pl.ANY)
    return pl.pallas_call(
        kernel,
        out_shape=jax.ShapeDtypeStruct(gate.shape, bf),
        in_specs=[hbm, vmem, vmem, vmem, hbm, hbm, vmem, vmem, vmem, vmem, vmem],
        out_specs=vmem,
        scratch_shapes=[
            pltpu.VMEM(kv_weight.shape, bf),
            pltpu.VMEM(queries.shape, bf),
            pltpu.VMEM(gate.shape, bf),
            pltpu.VMEM((16, rows, 256), jnp.float32),
            pltpu.VMEM((rows, rank), bf),
            pltpu.VMEM((ROPE, rows), bf),
            pltpu.VMEM((n_s // 2, 2, rows, rank), bf),
            pltpu.VMEM((n_s // 2, 2, ROPE, rows), bf),
            pltpu.VMEM((n_d, pairs, rows, PAIR), bf),
            pltpu.VMEM((heads, seq, KDIM), bf),
            pltpu.VMEM((heads, seq, 2 * VDIM), bf),
            pltpu.VMEM((n_d, pairs, rows, 2 * VDIM), bf),
            pltpu.VMEM((n_d, pairs, rows, 2 * VDIM), bf),
            dma, dma, dma, dma((2,)),
            dma((16, 5)), dma((16, 2)), dma((16, 5)), dma((16, 2)),
            *[dma((n_d, pairs))] * 4,
        ],
        compiler_params=pltpu.CompilerParams(
            has_side_effects=True, vmem_limit_bytes=60 * 1024 * 1024
        ),
        name="latent_attention",
    )(
        queries, latent, rope_key.T, latent_gain[None, :], kv_weight, gate, out_gain[None, :],
        *tables,
    )


def solution(mesh):
    return jax.shard_map(
        functools.partial(per_device, mesh.shape["sp"], mesh.shape["dp"]),
        mesh=mesh,
        in_specs=(
            P(("dp", "sp"), None),
            P(("dp", "sp"), None),
            P(("dp", "sp"), None),
            P(),
            P(None, "dp"),
            P(("dp", "sp"), None),
            P(),
        ),
        out_specs=P(("dp", "sp"), None),
        check_vma=False,
    )
```

time: 231 us -> 139 us (0.60)
  the two profiles are of different devices: /device:TPU:248 before, /device:TPU:159 now
where the time goes in v1:
time: 139 us
  Pallas kernels  137 us (99%)
  local copies, waits for them, and re-layouts  2.29 us (2%)
    pallas_call x1, Pallas kernels, per_device(): pl.pallas_call(kernel, out_shape=jax.ShapeDtypeStruct(gate.shape, bf), in...  137 us

profile of v1, /device:TPU:159, one launch (start us, length us, event | category | flops | bytes accessed | tf_op | source)
XLA Modules:
  0.0 139.0 jit_solution(8308758342844817372)
XLA Ops:
  0.0 136.7 %latent_attention.1 = bf16[128,4096]{1,0:T(8,128)(2,1)} custom-call(bf16[128,6144]{1,0:T(8,128)(2,1)} %q_ref.1, bf16[128,1024]{1,0:T(8,128)(2,1)} %lat_ref.1, bf16[64,128]{1,0:T(8,128)(2,1)} %bitcast.3, f32[1,1024]{1,0:T(1,128)} %bitcast.5, bf16[1024,1024]{1,0:T(8,128)(2,1)} %w_ref.1, bf16[128,4096]{1,0:T(8,128)(2,1)} %gate_ref.1, f32[1,4096]{1,0:T(1,128)} %bitcast.4, ...), custom_call_target="tpu_custom_call" | custom-call | tf_op jit(solution)/shard_map/latent_attention/pallas_call | solution.py:315
  136.7 2.3 %copy.13 = bf16[128,4096]{1,0:T(8,128)(2,1)} copy(bf16[128,4096]{1,0:T(8,128)(2,1)} %latent_attention.1) | data formatting | bytes 2097152

commit v2 on v1

--- a/solution.py
+++ b/solution.py
@@ -28,7 +28,13 @@
     (0, 0), (1, 0), (3, 0), (0, 3), (0, 1), (2, 0), (1, 3), (1, 1),
     (3, 1), (3, 3), (0, 2), (2, 1), (2, 3), (1, 2), (3, 2), (2, 2),
 )
-QUERIES_AT = 11
+WHOLE = (
+    (0, 0), (3, 0), (0, 3), (1, 0), (0, 1), (1, 1), (1, 3), (3, 1),
+    (3, 3), (0, 2), (2, 0), (2, 1), (1, 2), (2, 3), (3, 2), (2, 2),
+)
+DONE = (0, 1, 1, 1, 3, 5, 5, 5, 6, 8, 9, 11, 11, 11, 13, 15, 16)
+PIECES = ((0, 48), (48, 48), (96, 32))
+QUERIES_AT = (4, 9, 13, 16)
 
 
 def turn(x, cosine, sine, mask):
@@ -37,10 +43,10 @@
 
 
 def kernel(
-    q_ref, lat_ref, rk_ref, lgain_ref, w_ref, gate_ref, ogain_ref, ta_ref, tb_ref, ka_ref, kb_ref,
+    q_ref, lat_ref, rk_ref, lgain_ref, w_ref, gate_ref, ogain_ref, ta_ref, tb_ref, ka_ref,
     out_ref,
     w_v, q_v, gate_v, silu_v, own_lat, own_rk, latb, rkb, qb, kbuf, vbuf, ob, orecv,
-    w_sem, q_sem, gate_sem, own_send, lat_send, lat_recv, rk_send, rk_recv,
+    w_sem, q_sem, gate_sem, out_sem, own_send, lat_send, lat_recv, rk_send, rk_recv,
     q_send, q_recv, o_send, o_recv,
 ):
     s, d = lax.axis_index("sp"), lax.axis_index("dp")
@@ -78,6 +84,32 @@
     def arrived(dst, rsem):
         pltpu.make_async_copy(dst, dst, rsem).wait()
 
+    def piece(n):
+        return pl.ds(*PIECES[n])
+
+    column = (x + y + 2 * c) % 4
+    first_block = k * 4 + column
+    first_to = ((2 * k + c) * 4 + (x + c) % 4, 2 * column + par)
+    root_x = (y + 4 - par) % 4
+    root_from = ((2 * k + c) * 4 + (x + 4 - root_x + 2 * par) % 4, seq)
+    peers = [
+        (s, 2 * ((x + 1) % 4) + c), (s, 2 * ((x + 3) % 4) + c), (s, 2 * x + 1 - c),
+        (((z + 2) % 8) * 4 + y, d), (((z + 6) % 8) * 4 + y, d), first_to, root_from,
+        *[(k * 8 + home, jnp.int32(t)) for t in range(8)], *[(k * 8 + j, seq) for j in range(8)],
+    ]
+    barrier = pltpu.get_barrier_semaphore()
+    others = jnp.int32(0)
+    for ts, td in peers:
+        same = (ts == s) & (td == d)
+
+        @pl.when(jnp.logical_not(same))
+        def _():
+            pl.semaphore_signal(
+                barrier, inc=1, device_id={"sp": ts, "dp": td}, device_id_type=MESH
+            )
+
+        others = others + jnp.where(same, 0, 1)
+
     w_copy = pltpu.make_async_copy(w_ref, w_v, w_sem)
     q_copy = pltpu.make_async_copy(q_ref, q_v, q_sem)
     gate_copy = pltpu.make_async_copy(gate_ref, gate_v, gate_sem)
@@ -89,13 +121,27 @@
     scale = lax.rsqrt(jnp.mean(wide * wide, axis=-1, keepdims=True) + EPS)
     own_lat[...] = (wide * scale * lgain_ref[...]).astype(jnp.bfloat16)
     half = ROPE // 2
-    kca, ksa, kcb, ksb = ka_ref[0], ka_ref[1], kb_ref[0, s], kb_ref[1, s]
+    kca, ksa = ka_ref[0], ka_ref[1]
+    kcb, ksb = tb_ref[0, s][:, :half].T, tb_ref[1, s][:, :half].T
     kc, ks = kca * kcb - ksa * ksb, ksa * kcb + kca * ksb
     raw = rk_ref[...].astype(jnp.float32)
     u1, u2 = raw[:half], raw[half:]
     own_rk[:half] = (u1 * kc - u2 * ks).astype(jnp.bfloat16)
     own_rk[half:] = (u2 * kc + u1 * ks).astype(jnp.bfloat16)
 
+    pl.semaphore_wait(barrier, others)
+    own_sends = [
+        (
+            own_lat.at[piece(n)], latb.at[first_block, par, piece(n)], own_send.at[n],
+            lat_recv.at[first_block, par, n], *first_to,
+        )
+        for n in range(len(PIECES))
+    ] + [
+        (own_rk, rkb.at[first_block, par], own_send.at[len(PIECES)], rk_recv.at[first_block, par], *first_to),
+    ]
+    for args in own_sends:
+        send(*args)
+
     ones = jnp.ones((rows, 128), jnp.bfloat16)
 
     def ones_step(i, carry):
@@ -105,15 +151,6 @@
         return carry
 
     lax.fori_loop(0, vbuf.shape[1] // rows, ones_step, 0)
-
-    first_block = k * 4 + y
-    first_to = ((2 * k + c) * 4 + (x + c) % 4, 2 * y + par)
-    own_sends = [
-        (own_lat, latb.at[first_block, par], own_send.at[0], lat_recv.at[first_block, par], *first_to),
-        (own_rk, rkb.at[first_block, par], own_send.at[1], rk_recv.at[first_block, par], *first_to),
-    ]
-    for args in own_sends:
-        send(*args)
 
     lane = lax.broadcasted_iota(jnp.int32, (rows, 128), 1)
     mask = (lane % 64) < 32
@@ -129,14 +166,19 @@
         q_v[:, at] = turn(
             q_v[:, at].astype(jnp.float32), cosine_high, sine_high, mask
         ).astype(jnp.bfloat16)
-    query_sends = [
-        (
-            q_v.at[:, pl.ds((t * pairs + p) * PAIR, PAIR)], qb.at[m, p],
-            q_send.at[t, p], q_recv.at[m, p], k * 8 + home, jnp.int32(t),
-        )
-        for p in range(pairs)
-        for t in range(8)
-    ]
+
+    def query_sends(turn):
+        sends = []
+        for p in range(pairs):
+            for core in range(2):
+                t = 2 * ((x + m // 2 + 4 - turn) % 4) + core
+                cols = pl.ds(pl.multiple_of((t * pairs + p) * PAIR, PAIR), PAIR)
+                sends.append((
+                    q_v.at[:, cols], qb.at[m, p],
+                    q_send.at[2 * turn + core, p], q_recv.at[m, p], k * 8 + home, t,
+                ))
+        return sends
+
     gate_copy.wait()
     for i in range(16):
         at = slice(i * 256, (i + 1) * 256)
@@ -146,28 +188,48 @@
 
     low = lax.broadcasted_iota(jnp.int32, (2 * rows, 128), 1) < 64
 
-    def place(i):
+    def place(i, order=ORDER):
         dk, dx = jnp.int32(0), jnp.int32(0)
-        for n, (a, b) in enumerate(ORDER):
+        for n, (a, b) in enumerate(order):
             dk = jnp.where(i == n, a, dk)
             dx = jnp.where(i == n, b, dx)
-        return dk, dx, ((k + dk) % 4) * 4 + (x + dx) % 4
-
-    def forwards(i, act):
-        dk, dx, block = place(i)
-        own = dx == 0
+        return dk, dx
+
+    def block_at(dk, dx):
+        return ((k + dk) % 4) * 4 + (x + dx) % 4
+
+    last = len(PIECES) - 1
+
+    def part_place(i, part):
+        first, second = place(i)
+        return (second, first) if part == last else (first, second)
+
+    def forwards(i, part, act):
+        first, second = place(i)
+        block = block_at(*part_place(i, part))
+        own = second == 0
+        ahead = own | ((second == 3) & (first < 2))
+        back = own | ((second == 1) & (first >= 2))
+        ahead_first = own & ((first == 0) | ((first == 3) & (c == 0)))
+        back_first = own & ((first == 0) | ((first == 1) & (c == 1)))
+        along_x, along_z = (ahead, back), (ahead_first, back_first)
+        if part == last:
+            along_x, along_z = along_z, along_x
         ways = (
-            (own | ((dx == 3) & (dk < 2)), s, 2 * ((x + 1) % 4) + c),
-            (own | ((dx == 1) & (dk >= 2)), s, 2 * ((x + 3) % 4) + c),
-            (own & ((dk == 0) | ((dk == 3) & (c == 0))), ((z + 2) % 8) * 4 + y, d),
-            (own & ((dk == 0) | ((dk == 1) & (c == 1))), ((z + 6) % 8) * 4 + y, d),
+            (along_x[0], s, 2 * ((x + 1) % 4) + c),
+            (along_x[1], s, 2 * ((x + 3) % 4) + c),
+            (along_z[0], ((z + 2) % 8) * 4 + y, d),
+            (along_z[1], ((z + 6) % 8) * 4 + y, d),
             (None, s, 2 * x + 1 - c),
         )
+        blocks = [(latb.at[block, c, piece(part)], lat_send.at[i, part], lat_recv.at[block, c, part])]
+        if part == 0:
+            blocks.append((rkb.at[block, c], rk_send.at[i], rk_recv.at[block, c]))
         for n, (when, ts, td) in enumerate(ways):
             def go(n=n, ts=ts, td=td):
-                for buf, ssem, rsem in ((latb, lat_send, lat_recv), (rkb, rk_send, rk_recv)):
+                for buf, ssem, rsem in blocks:
                     act(pltpu.make_async_remote_copy(
-                        buf.at[block, c], buf.at[block, c], ssem.at[i, n], rsem.at[block, c],
+                        buf, buf, ssem.at[n], rsem,
                         device_id={"sp": ts, "dp": td}, device_id_type=MESH,
                     ))
 
@@ -176,19 +238,41 @@
             else:
                 pl.when(when)(go)
 
+    def landed(block, core):
+        for n in range(len(PIECES)):
+            arrived(latb.at[block, core, piece(n)], lat_recv.at[block, core, n])
+        arrived(rkb.at[block, core], rk_recv.at[block, core])
+
+    def send_queries(i):
+        for turn in range(4):
+            @pl.when(i == QUERIES_AT[turn])
+            def _():
+                for args in query_sends(turn):
+                    send(*args)
+
+    def take(i):
+        for n in range(len(PIECES)):
+            block = block_at(*part_place(i, n))
+            arrived(latb.at[block, c, piece(n)], lat_recv.at[block, c, n])
+            if n == 0:
+                arrived(rkb.at[block, c], rk_recv.at[block, c])
+            forwards(i, n, lambda copy: copy.start())
+
     def key_step(i, carry):
-        _, _, block = place(i)
-        arrived(latb.at[block, c], lat_recv.at[block, c])
-        arrived(rkb.at[block, c], rk_recv.at[block, c])
-        forwards(i, lambda copy: copy.start())
-
-        @pl.when(i == QUERIES_AT)
+        @pl.when(i < 16)
         def _():
-            for args in query_sends:
-                send(*args)
-
-        arrived(latb.at[block, 1 - c], lat_recv.at[block, 1 - c])
-        arrived(rkb.at[block, 1 - c], rk_recv.at[block, 1 - c])
+            take(i)
+
+        send_queries(i)
+        start, stop = jnp.int32(0), jnp.int32(0)
+        for n in range(1, len(DONE)):
+            start = jnp.where(i == n, DONE[n - 1], start)
+            stop = jnp.where(i == n, DONE[n], stop)
+        return lax.fori_loop(start, stop, whole_step, carry)
+
+    def whole_step(i, carry):
+        block = block_at(*place(i, WHOLE))
+        landed(block, 1 - c)
         at = pl.ds(pl.multiple_of(i * 2 * rows, 2 * rows), 2 * rows)
         normed = latb[block].reshape(2 * rows, lat_ref.shape[1])
         both_rk = jnp.concatenate([rkb[block, 0], rkb[block, 1]], axis=1).astype(jnp.float32)
@@ -210,7 +294,8 @@
             vbuf[h, at, :VDIM] = both[:, NOPE:].astype(jnp.bfloat16)
         return carry
 
-    lax.fori_loop(0, 16, key_step, 0)
+    take(jnp.int32(0))
+    lax.fori_loop(1, len(DONE), key_step, 0)
 
     factor = LOG2E * QDIM ** -0.5
     n_chunks = kbuf.shape[1] // CHUNK
@@ -219,7 +304,7 @@
         return (ob.at[j, p], orecv.at[d, p], o_send.at[j, p], o_recv.at[d, p], k * 8 + j, seq)
 
     def query_step(i, carry):
-        r, p = (i // pairs + m // 2) % 4, i % pairs
+        r, p = (i // pairs + x + 4 - root_x) % 4, i % pairs
         for part in range(2):
             arrived(qb.at[2 * r + part, p], q_recv.at[2 * r + part, p])
         for odd in range(2):
@@ -256,6 +341,16 @@
 
     lax.fori_loop(0, 4 * pairs, query_step, 0)
 
+    for args in sum(map(query_sends, range(4)), own_sends):
+        sent(*args)
+
+    def forwards_sent(i, carry):
+        for n in range(len(PIECES)):
+            forwards(i, n, lambda copy: copy.wait_send())
+        return carry
+
+    lax.fori_loop(0, 16, forwards_sent, 0)
+
     square = jnp.zeros((rows, 1), jnp.float32)
     for p in range(pairs):
         for t in range(8):
@@ -264,24 +359,24 @@
             silu_v[t * pairs + p] = gated
             square = square + jnp.sum(gated * gated, axis=-1, keepdims=True)
     scale = lax.rsqrt(square / (HEADS * VDIM) + EPS)
+    outs = []
     for i in range(16):
         cols = slice(i * 256, (i + 1) * 256)
-        out_ref[:, cols] = (silu_v[i] * scale * ogain_ref[:, cols]).astype(jnp.bfloat16)
-
-    for args in own_sends + query_sends:
-        sent(*args)
-
-    def forwards_sent(i, carry):
-        forwards(i, lambda copy: copy.wait_send())
-        return carry
-
-    lax.fori_loop(0, 16, forwards_sent, 0)
+        gate_v[:, cols] = (silu_v[i] * scale * ogain_ref[:, cols]).astype(jnp.bfloat16)
+        if i % 4 == 3:
+            cols = pl.ds(i // 4 * 1024, 1024)
+            outs.append(
+                pltpu.make_async_copy(gate_v.at[:, cols], out_ref.at[:, cols], out_sem.at[i // 4])
+            )
+            outs[-1].start()
 
     def output_sent(i, carry):
         sent(*output_send(i // pairs, i % pairs))
         return carry
 
     lax.fori_loop(0, 8 * pairs, output_sent, 0)
+    for copy in outs:
+        copy.wait()
 
 
 def angle_tables(rows, n_s):
@@ -298,7 +393,6 @@
         both(inner[:, None] * inverse[None, :]),
         both(outer[:, None] * inverse[None, :])[:, :, None, :],
         both(base[:, None] * inner[None, :]),
-        both(outer[:, None] * base[None, :])[:, :, :, None],
     )
 
 
@@ -315,8 +409,8 @@
     return pl.pallas_call(
         kernel,
         out_shape=jax.ShapeDtypeStruct(gate.shape, bf),
-        in_specs=[hbm, vmem, vmem, vmem, hbm, hbm, vmem, vmem, vmem, vmem, vmem],
-        out_specs=vmem,
+        in_specs=[hbm, vmem, vmem, vmem, hbm, hbm, vmem, vmem, vmem, vmem],
+        out_specs=hbm,
         scratch_shapes=[
             pltpu.VMEM(kv_weight.shape, bf),
             pltpu.VMEM(queries.shape, bf),
@@ -331,12 +425,12 @@
             pltpu.VMEM((heads, seq, 2 * VDIM), bf),
             pltpu.VMEM((n_d, pairs, rows, 2 * VDIM), bf),
             pltpu.VMEM((n_d, pairs, rows, 2 * VDIM), bf),
-            dma, dma, dma, dma((2,)),
-            dma((16, 5)), dma((16, 2)), dma((16, 5)), dma((16, 2)),
+            dma, dma, dma, dma((4,)), dma((len(PIECES) + 1,)),
+            dma((16, len(PIECES), 5)), dma((16, 2, len(PIECES))), dma((16, 5)), dma((16, 2)),
             *[dma((n_d, pairs))] * 4,
         ],
         compiler_params=pltpu.CompilerParams(
-            has_side_effects=True, vmem_limit_bytes=60 * 1024 * 1024
+            has_side_effects=True, collective_id=0, vmem_limit_bytes=60 * 1024 * 1024
         ),
         name="latent_attention",
     )(

time: 139 us -> 119 us (0.86)
  the two profiles are of different devices: /device:TPU:159 before, /device:TPU:24 now
where the time goes in v2:
time: 119 us; the launch traced here: 117 us
  Pallas kernels  115 us (97%)
  local copies, waits for them, and re-layouts  2.29 us (2%)
    pallas_call x1, Pallas kernels, per_device(): pl.pallas_call(kernel, out_shape=jax.ShapeDtypeStruct(gate.shape, bf), in...  115 us

profile of v2, /device:TPU:24, one launch (start us, length us, event | category | flops | bytes accessed | tf_op | source)
XLA Modules:
  0.0 117.4 jit_solution(9975557279361403768)
XLA Ops:
  0.0 115.1 %latent_attention.1 = bf16[128,4096]{1,0:T(8,128)(2,1)} custom-call(bf16[128,6144]{1,0:T(8,128)(2,1)} %q_ref.1, bf16[128,1024]{1,0:T(8,128)(2,1)} %lat_ref.1, bf16[64,128]{1,0:T(8,128)(2,1)} %bitcast.3, f32[1,1024]{1,0:T(1,128)} %bitcast.5, bf16[1024,1024]{1,0:T(8,128)(2,1)} %w_ref.1, bf16[128,4096]{1,0:T(8,128)(2,1)} %gate_ref.1, f32[1,4096]{1,0:T(1,128)} %bitcast.4, ...), custom_call_target="tpu_custom_call" | custom-call | tf_op jit(solution)/shard_map/latent_attention/pallas_call | solution.py:409
  115.1 2.3 %copy.12 = bf16[128,4096]{1,0:T(8,128)(2,1)} copy(bf16[128,4096]{1,0:T(8,128)(2,1)} %latent_attention.1) | data formatting | bytes 2097152

commit v3 on v2

--- a/solution.py
+++ b/solution.py
@@ -34,7 +34,7 @@
 )
 DONE = (0, 1, 1, 1, 3, 5, 5, 5, 6, 8, 9, 11, 11, 11, 13, 15, 16)
 PIECES = ((0, 48), (48, 48), (96, 32))
-QUERIES_AT = (4, 9, 13, 16)
+QUERIES_AT = (0, 4, 8, 12)
 
 
 def turn(x, cosine, sine, mask):
@@ -55,9 +55,9 @@
     x, c = d // 2, d % 2
     k, par = z // 2, z % 2
     m = par * 4 + y
-    seq = 2 * ((y + 4 - par) % 4) + par
-    home = c * 4 + (x + c) % 4
-    pairs = 2
+    seq = 2 * ((y + 4 - 2 * par) % 4) + par
+    home = c * 4 + (x + 2 * c) % 4
+    pairs, heads = 2, 4
 
     def send(src, dst, ssem, rsem, ts, td):
         same = (ts == s) & (td == d)
@@ -89,8 +89,8 @@
 
     column = (x + y + 2 * c) % 4
     first_block = k * 4 + column
-    first_to = ((2 * k + c) * 4 + (x + c) % 4, 2 * column + par)
-    root_x = (y + 4 - par) % 4
+    first_to = ((2 * k + c) * 4 + (x + 2 * c) % 4, 2 * column + par)
+    root_x = (y + 4 - 2 * par) % 4
     root_from = ((2 * k + c) * 4 + (x + 4 - root_x + 2 * par) % 4, seq)
     peers = [
         (s, 2 * ((x + 1) % 4) + c), (s, 2 * ((x + 3) % 4) + c), (s, 2 * x + 1 - c),
@@ -132,12 +132,12 @@
     pl.semaphore_wait(barrier, others)
     own_sends = [
         (
-            own_lat.at[piece(n)], latb.at[first_block, par, piece(n)], own_send.at[n],
+            own_lat.at[piece(n)], latb.at[2 * first_block + par, piece(n)], own_send.at[n],
             lat_recv.at[first_block, par, n], *first_to,
         )
         for n in range(len(PIECES))
     ] + [
-        (own_rk, rkb.at[first_block, par], own_send.at[len(PIECES)], rk_recv.at[first_block, par], *first_to),
+        (own_rk, rkb.at[2 * first_block + par], own_send.at[len(PIECES)], rk_recv.at[first_block, par], *first_to),
     ]
     for args in own_sends:
         send(*args)
@@ -180,8 +180,8 @@
         return sends
 
     gate_copy.wait()
-    for i in range(16):
-        at = slice(i * 256, (i + 1) * 256)
+    for i in range(HEADS):
+        at = slice(i * VDIM, (i + 1) * VDIM)
         g = gate_v[:, at].astype(jnp.float32)
         silu_v[i] = g / (1.0 + jnp.exp(-g))
     w_copy.wait()
@@ -204,7 +204,7 @@
         first, second = place(i)
         return (second, first) if part == last else (first, second)
 
-    def forwards(i, part, act):
+    def forwards(i, part):
         first, second = place(i)
         block = block_at(*part_place(i, part))
         own = second == 0
@@ -222,16 +222,16 @@
             (along_z[1], ((z + 6) % 8) * 4 + y, d),
             (None, s, 2 * x + 1 - c),
         )
-        blocks = [(latb.at[block, c, piece(part)], lat_send.at[i, part], lat_recv.at[block, c, part])]
+        blocks = [(latb.at[2 * block + c, piece(part)], lat_send, lat_recv.at[block, c, part])]
         if part == 0:
-            blocks.append((rkb.at[block, c], rk_send.at[i], rk_recv.at[block, c]))
-        for n, (when, ts, td) in enumerate(ways):
-            def go(n=n, ts=ts, td=td):
+            blocks.append((rkb.at[2 * block + c], rk_send, rk_recv.at[block, c]))
+        for when, ts, td in ways:
+            def go(ts=ts, td=td):
                 for buf, ssem, rsem in blocks:
-                    act(pltpu.make_async_remote_copy(
-                        buf, buf, ssem.at[n], rsem,
+                    pltpu.make_async_remote_copy(
+                        buf, buf, ssem, rsem,
                         device_id={"sp": ts, "dp": td}, device_id_type=MESH,
-                    ))
+                    ).start()
 
             if when is None:
                 go()
@@ -240,8 +240,8 @@
 
     def landed(block, core):
         for n in range(len(PIECES)):
-            arrived(latb.at[block, core, piece(n)], lat_recv.at[block, core, n])
-        arrived(rkb.at[block, core], rk_recv.at[block, core])
+            arrived(latb.at[2 * block + core, piece(n)], lat_recv.at[block, core, n])
+        arrived(rkb.at[2 * block + core], rk_recv.at[block, core])
 
     def send_queries(i):
         for turn in range(4):
@@ -250,32 +250,69 @@
                 for args in query_sends(turn):
                     send(*args)
 
-    def take(i):
-        for n in range(len(PIECES)):
-            block = block_at(*part_place(i, n))
-            arrived(latb.at[block, c, piece(n)], lat_recv.at[block, c, n])
-            if n == 0:
-                arrived(rkb.at[block, c], rk_recv.at[block, c])
-            forwards(i, n, lambda copy: copy.start())
+    def take(i, part):
+        block = block_at(*part_place(i, part))
+        arrived(latb.at[2 * block + c, piece(part)], lat_recv.at[block, c, part])
+        if part == 0:
+            arrived(rkb.at[2 * block + c], rk_recv.at[block, c])
+        forwards(i, part)
 
     def key_step(i, carry):
         @pl.when(i < 16)
         def _():
-            take(i)
+            for part in range(len(PIECES)):
+                take(i, part)
 
         send_queries(i)
+        lax.fori_loop(*between(DONE, i), whole_step, 0)
+        return carry
+
+    def between(table, i):
         start, stop = jnp.int32(0), jnp.int32(0)
-        for n in range(1, len(DONE)):
-            start = jnp.where(i == n, DONE[n - 1], start)
-            stop = jnp.where(i == n, DONE[n], stop)
-        return lax.fori_loop(start, stop, whole_step, carry)
+        for n in range(1, len(table)):
+            start = jnp.where(i == n, table[n - 1], start)
+            stop = jnp.where(i == n, table[n], stop)
+        return start, stop
+
+    factor = LOG2E * QDIM ** -0.5
+    n_chunks = kbuf.shape[1] // CHUNK
+
+    def step_place(i):
+        return (i // pairs + x + 4 - root_x) % 4, i % pairs
+
+    def attend(i, odd, chunks, total, before):
+        r, p = step_place(i)
+        h = 2 * p + odd
+        at = slice(odd * 128, odd * 128 + KDIM)
+        q = jnp.concatenate([qb[2 * r, p, :, at], qb[2 * r + 1, p, :, at]], axis=0)
+
+        def score(j):
+            return lax.dot_general(
+                q, kbuf[h, j * CHUNK : (j + 1) * CHUNK], DN_T, preferred_element_type=jnp.float32
+            )
+
+        following = score(chunks[0])
+        for j in chunks:
+            scores = following
+            if j != chunks[-1]:
+                following = score(j + 1)
+            top = jnp.max(scores, axis=-1, keepdims=True)
+            if before is not None:
+                top = jnp.maximum(top, before)
+            raised = jnp.exp2((scores - top) * factor).astype(jnp.bfloat16)
+            part_total = jnp.dot(
+                raised, vbuf[h, j * CHUNK : (j + 1) * CHUNK], preferred_element_type=jnp.float32
+            )
+            total = part_total if before is None else total * jnp.exp2((before - top) * factor) + part_total
+            before = top
+        return total, before
 
     def whole_step(i, carry):
         block = block_at(*place(i, WHOLE))
         landed(block, 1 - c)
         at = pl.ds(pl.multiple_of(i * 2 * rows, 2 * rows), 2 * rows)
-        normed = latb[block].reshape(2 * rows, lat_ref.shape[1])
-        both_rk = jnp.concatenate([rkb[block, 0], rkb[block, 1]], axis=1).astype(jnp.float32)
+        normed = latb[pl.ds(2 * block, 2)].reshape(2 * rows, lat_ref.shape[1])
+        both_rk = jnp.concatenate([rkb[2 * block], rkb[2 * block + 1]], axis=1).astype(jnp.float32)
         rot = jnp.concatenate([both_rk, jnp.zeros_like(both_rk)], axis=0).T
         rot_high = pltpu.roll(rot, 64, 1)
         for h in range(4):
@@ -294,87 +331,62 @@
             vbuf[h, at, :VDIM] = both[:, NOPE:].astype(jnp.bfloat16)
         return carry
 
-    take(jnp.int32(0))
+    for part in range(len(PIECES)):
+        take(jnp.int32(0), part)
+    send_queries(jnp.int32(0))
     lax.fori_loop(1, len(DONE), key_step, 0)
 
-    factor = LOG2E * QDIM ** -0.5
-    n_chunks = kbuf.shape[1] // CHUNK
-
-    def output_send(j, p):
-        return (ob.at[j, p], orecv.at[d, p], o_send.at[j, p], o_recv.at[d, p], k * 8 + j, seq)
-
-    def query_step(i, carry):
-        r, p = (i // pairs + x + 4 - root_x) % 4, i % pairs
+    def output_send(j, h):
+        return (ob.at[j, h], orecv.at[d, h], o_send.at[j, h], o_recv.at[d, h], k * 8 + j, seq)
+
+    def query_step(i, carry, split=False):
+        r, p = step_place(i)
         for part in range(2):
             arrived(qb.at[2 * r + part, p], q_recv.at[2 * r + part, p])
         for odd in range(2):
-            h = 2 * p + odd
-            at = slice(odd * 128, odd * 128 + KDIM)
-            q = jnp.concatenate([qb[2 * r, p, :, at], qb[2 * r + 1, p, :, at]], axis=0)
-
-            def score(j):
-                return lax.dot_general(
-                    q, kbuf[h, j * CHUNK : (j + 1) * CHUNK], DN_T, preferred_element_type=jnp.float32
-                )
-
-            following = score(0)
-            for j in range(n_chunks):
-                scores = following
-                if j + 1 < n_chunks:
-                    following = score(j + 1)
-                top = jnp.max(scores, axis=-1, keepdims=True)
-                if j:
-                    top = jnp.maximum(top, before)
-                raised = jnp.exp2((scores - top) * factor).astype(jnp.bfloat16)
-                part_total = jnp.dot(
-                    raised, vbuf[h, j * CHUNK : (j + 1) * CHUNK], preferred_element_type=jnp.float32
-                )
-                total = total * jnp.exp2((before - top) * factor) + part_total if j else part_total
-                before = top
+            total, _ = attend(i, odd, range(n_chunks), None, None)
             result = (total[:, :VDIM] / total[:, VDIM:]).astype(jnp.bfloat16)
-            at = slice(odd * VDIM, (odd + 1) * VDIM)
-            ob[2 * r, p, :, at] = result[:rows]
-            ob[2 * r + 1, p, :, at] = result[rows:]
-        send(*output_send(2 * r, p))
-        send(*output_send(2 * r + 1, p))
+            ob[2 * r, 2 * p + odd] = result[:rows]
+            ob[2 * r + 1, 2 * p + odd] = result[rows:]
+            if split or odd:
+                for h in (2 * p + odd,) if split else (2 * p, 2 * p + 1):
+                    send(*output_send(2 * r, h))
+                    send(*output_send(2 * r + 1, h))
         return carry
 
-    lax.fori_loop(0, 4 * pairs, query_step, 0)
+    lax.fori_loop(0, 4 * pairs - 1, query_step, 0)
+    query_step(jnp.int32(4 * pairs - 1), 0, True)
 
     for args in sum(map(query_sends, range(4)), own_sends):
         sent(*args)
 
-    def forwards_sent(i, carry):
-        for n in range(len(PIECES)):
-            forwards(i, n, lambda copy: copy.wait_send())
-        return carry
-
-    lax.fori_loop(0, 16, forwards_sent, 0)
+    arrived(latb.at[pl.ds(0, 31)], lat_send)
+    arrived(rkb.at[pl.ds(0, 31)], rk_send)
 
     square = jnp.zeros((rows, 1), jnp.float32)
-    for p in range(pairs):
+    for h in range(4):
         for t in range(8):
-            arrived(orecv.at[t, p], o_recv.at[t, p])
-            gated = orecv[t, p].astype(jnp.float32) * silu_v[t * pairs + p]
-            silu_v[t * pairs + p] = gated
+            arrived(orecv.at[t, h], o_recv.at[t, h])
+            gated = orecv[t, h].astype(jnp.float32) * silu_v[t * 4 + h]
+            silu_v[t * 4 + h] = gated
             square = square + jnp.sum(gated * gated, axis=-1, keepdims=True)
     scale = lax.rsqrt(square / (HEADS * VDIM) + EPS)
     outs = []
-    for i in range(16):
-        cols = slice(i * 256, (i + 1) * 256)
+    for i in range(HEADS):
+        cols = slice(i * VDIM, (i + 1) * VDIM)
         gate_v[:, cols] = (silu_v[i] * scale * ogain_ref[:, cols]).astype(jnp.bfloat16)
-        if i % 4 == 3:
-            cols = pl.ds(i // 4 * 1024, 1024)
+        if i % 8 == 7:
+            cols = pl.ds(i // 8 * 1024, 1024)
             outs.append(
-                pltpu.make_async_copy(gate_v.at[:, cols], out_ref.at[:, cols], out_sem.at[i // 4])
+                pltpu.make_async_copy(gate_v.at[:, cols], out_ref.at[:, cols], out_sem.at[i // 8])
             )
             outs[-1].start()
 
     def output_sent(i, carry):
-        sent(*output_send(i // pairs, i % pairs))
+        sent(*output_send(i // heads, i % heads))
         return carry
 
-    lax.fori_loop(0, 8 * pairs, output_sent, 0)
+    lax.fori_loop(0, 8 * heads, output_sent, 0)
     for copy in outs:
         copy.wait()
 
@@ -415,19 +427,19 @@
             pltpu.VMEM(kv_weight.shape, bf),
             pltpu.VMEM(queries.shape, bf),
             pltpu.VMEM(gate.shape, bf),
-            pltpu.VMEM((16, rows, 256), jnp.float32),
+            pltpu.VMEM((HEADS, rows, VDIM), jnp.float32),
             pltpu.VMEM((rows, rank), bf),
             pltpu.VMEM((ROPE, rows), bf),
-            pltpu.VMEM((n_s // 2, 2, rows, rank), bf),
-            pltpu.VMEM((n_s // 2, 2, ROPE, rows), bf),
+            pltpu.VMEM((n_s, rows, rank), bf),
+            pltpu.VMEM((n_s, ROPE, rows), bf),
             pltpu.VMEM((n_d, pairs, rows, PAIR), bf),
             pltpu.VMEM((heads, seq, KDIM), bf),
             pltpu.VMEM((heads, seq, 2 * VDIM), bf),
-            pltpu.VMEM((n_d, pairs, rows, 2 * VDIM), bf),
-            pltpu.VMEM((n_d, pairs, rows, 2 * VDIM), bf),
+            pltpu.VMEM((n_d, heads, rows, VDIM), bf),
+            pltpu.VMEM((n_d, heads, rows, VDIM), bf),
             dma, dma, dma, dma((4,)), dma((len(PIECES) + 1,)),
-            dma((16, len(PIECES), 5)), dma((16, 2, len(PIECES))), dma((16, 5)), dma((16, 2)),
-            *[dma((n_d, pairs))] * 4,
+            dma, dma((16, 2, len(PIECES))), dma, dma((16, 2)),
+            *[dma((n_d, pairs))] * 2, *[dma((n_d, heads))] * 2,
         ],
         compiler_params=pltpu.CompilerParams(
             has_side_effects=True, collective_id=0, vmem_limit_bytes=60 * 1024 * 1024

time: 119 us -> 113 us (0.950); the launches traced: 117 us -> 113 us
  Pallas kernels: 115 us -> 111 us
    pallas_call x1, Pallas kernels: 115 us -> 111 us  [per_device(): pl.pallas_call(kernel, out_shape=jax.ShapeDtypeStruct(gate.shape, bf), in...]
where the time goes in v3:
time: 113 us
  Pallas kernels  111 us (98%)
  local copies, waits for them, and re-layouts  2.29 us (2%)
    pallas_call x1, Pallas kernels, per_device(): pl.pallas_call(kernel, out_shape=jax.ShapeDtypeStruct(gate.shape, bf), in...  111 us
    unnamed x1, local copies, waits for them, and re-layouts  2.29 us

profile of v3, /device:TPU:24, one launch (start us, length us, event | category | flops | bytes accessed | tf_op | source)
XLA Modules:
  0.0 113.3 jit_solution(3715976432598023624)
XLA Ops:
  0.0 111.0 %latent_attention.1 = bf16[128,4096]{1,0:T(8,128)(2,1)} custom-call(bf16[128,6144]{1,0:T(8,128)(2,1)} %q_ref.1, bf16[128,1024]{1,0:T(8,128)(2,1)} %lat_ref.1, bf16[64,128]{1,0:T(8,128)(2,1)} %bitcast.3, f32[1,1024]{1,0:T(1,128)} %bitcast.5, bf16[1024,1024]{1,0:T(8,128)(2,1)} %w_ref.1, bf16[128,4096]{1,0:T(8,128)(2,1)} %gate_ref.1, f32[1,4096]{1,0:T(1,128)} %bitcast.4, ...), custom_call_target="tpu_custom_call" | custom-call | tf_op jit(solution)/shard_map/latent_attention/pallas_call | solution.py:421
  111.0 2.3 %copy.12 = bf16[128,4096]{1,0:T(8,128)(2,1)} copy(bf16[128,4096]{1,0:T(8,128)(2,1)} %latent_attention.1) | data formatting | bytes 2097152

commit v4 on v3

--- a/solution.py
+++ b/solution.py
@@ -32,9 +32,9 @@
     (0, 0), (3, 0), (0, 3), (1, 0), (0, 1), (1, 1), (1, 3), (3, 1),
     (3, 3), (0, 2), (2, 0), (2, 1), (1, 2), (2, 3), (3, 2), (2, 2),
 )
-DONE = (0, 1, 1, 1, 3, 5, 5, 5, 6, 8, 9, 11, 11, 11, 13, 15, 16)
+DONE = (0, 1, 1, 1, 3, 5, 5, 5, 6, 8, 9, 11, 11, 11, 15, 16)
 PIECES = ((0, 48), (48, 48), (96, 32))
-QUERIES_AT = (0, 4, 8, 12)
+QUERIES_AT = (0, 3, 7, 15)
 
 
 def turn(x, cosine, sine, mask):
@@ -46,7 +46,7 @@
     q_ref, lat_ref, rk_ref, lgain_ref, w_ref, gate_ref, ogain_ref, ta_ref, tb_ref, ka_ref,
     out_ref,
     w_v, q_v, gate_v, silu_v, own_lat, own_rk, latb, rkb, qb, kbuf, vbuf, ob, orecv,
-    w_sem, q_sem, gate_sem, out_sem, own_send, lat_send, lat_recv, rk_send, rk_recv,
+    w_sem, q_sem, gate_sem, out_sem, own_send, lat_send, lat_recv, partner_recv, rk_send, rk_recv,
     q_send, q_recv, o_send, o_recv,
 ):
     s, d = lax.axis_index("sp"), lax.axis_index("dp")
@@ -133,7 +133,7 @@
     own_sends = [
         (
             own_lat.at[piece(n)], latb.at[2 * first_block + par, piece(n)], own_send.at[n],
-            lat_recv.at[first_block, par, n], *first_to,
+            lat_recv.at[first_block, n], *first_to,
         )
         for n in range(len(PIECES))
     ] + [
@@ -175,7 +175,7 @@
                 cols = pl.ds(pl.multiple_of((t * pairs + p) * PAIR, PAIR), PAIR)
                 sends.append((
                     q_v.at[:, cols], qb.at[m, p],
-                    q_send.at[2 * turn + core, p], q_recv.at[m, p], k * 8 + home, t,
+                    q_send, q_recv.at[m, p], k * 8 + home, t,
                 ))
         return sends
 
@@ -222,12 +222,14 @@
             (along_z[1], ((z + 6) % 8) * 4 + y, d),
             (None, s, 2 * x + 1 - c),
         )
-        blocks = [(latb.at[2 * block + c, piece(part)], lat_send, lat_recv.at[block, c, part])]
+        blocks = [(latb.at[2 * block + c, piece(part)], lat_send, lat_recv.at[block, part])]
         if part == 0:
             blocks.append((rkb.at[2 * block + c], rk_send, rk_recv.at[block, c]))
         for when, ts, td in ways:
-            def go(ts=ts, td=td):
+            def go(ts=ts, td=td, when=when):
                 for buf, ssem, rsem in blocks:
+                    if when is None and ssem is lat_send:
+                        rsem = partner_recv.at[block]
                     pltpu.make_async_remote_copy(
                         buf, buf, ssem, rsem,
                         device_id={"sp": ts, "dp": td}, device_id_type=MESH,
@@ -239,8 +241,7 @@
                 pl.when(when)(go)
 
     def landed(block, core):
-        for n in range(len(PIECES)):
-            arrived(latb.at[2 * block + core, piece(n)], lat_recv.at[block, core, n])
+        arrived(latb.at[2 * block + core], partner_recv.at[block])
         arrived(rkb.at[2 * block + core], rk_recv.at[block, core])
 
     def send_queries(i):
@@ -252,17 +253,14 @@
 
     def take(i, part):
         block = block_at(*part_place(i, part))
-        arrived(latb.at[2 * block + c, piece(part)], lat_recv.at[block, c, part])
+        arrived(latb.at[2 * block + c, piece(part)], lat_recv.at[block, part])
         if part == 0:
             arrived(rkb.at[2 * block + c], rk_recv.at[block, c])
         forwards(i, part)
 
     def key_step(i, carry):
-        @pl.when(i < 16)
-        def _():
-            for part in range(len(PIECES)):
-                take(i, part)
-
+        for part in range(len(PIECES)):
+            take(i, part)
         send_queries(i)
         lax.fori_loop(*between(DONE, i), whole_step, 0)
         return carry
@@ -337,7 +335,7 @@
     lax.fori_loop(1, len(DONE), key_step, 0)
 
     def output_send(j, h):
-        return (ob.at[j, h], orecv.at[d, h], o_send.at[j, h], o_recv.at[d, h], k * 8 + j, seq)
+        return (ob.at[j, h], orecv.at[d, h], o_send, o_recv.at[d, h], k * 8 + j, seq)
 
     def query_step(i, carry, split=False):
         r, p = step_place(i)
@@ -357,8 +355,19 @@
     lax.fori_loop(0, 4 * pairs - 1, query_step, 0)
     query_step(jnp.int32(4 * pairs - 1), 0, True)
 
-    for args in sum(map(query_sends, range(4)), own_sends):
+    for args in own_sends:
         sent(*args)
+
+    def all_sent(buf, sem, same):
+        @pl.when(jnp.logical_not(same))
+        def _():
+            arrived(buf, sem)
+
+        @pl.when(same)
+        def _():
+            arrived(buf.at[pl.ds(0, 7)], sem)
+
+    all_sent(qb, q_send, home == m)
 
     arrived(latb.at[pl.ds(0, 31)], lat_send)
     arrived(rkb.at[pl.ds(0, 31)], rk_send)
@@ -382,11 +391,7 @@
             )
             outs[-1].start()
 
-    def output_sent(i, carry):
-        sent(*output_send(i // heads, i % heads))
-        return carry
-
-    lax.fori_loop(0, 8 * heads, output_sent, 0)
+    all_sent(ob, o_send, seq == d)
     for copy in outs:
         copy.wait()
 
@@ -438,8 +443,8 @@
             pltpu.VMEM((n_d, heads, rows, VDIM), bf),
             pltpu.VMEM((n_d, heads, rows, VDIM), bf),
             dma, dma, dma, dma((4,)), dma((len(PIECES) + 1,)),
-            dma, dma((16, 2, len(PIECES))), dma, dma((16, 2)),
-            *[dma((n_d, pairs))] * 2, *[dma((n_d, heads))] * 2,
+            dma, dma((16, len(PIECES))), dma((16,)), dma, dma((16, 2)),
+            dma, dma((n_d, pairs)), dma, dma((n_d, heads)),
         ],
         compiler_params=pltpu.CompilerParams(
             has_side_effects=True, collective_id=0, vmem_limit_bytes=60 * 1024 * 1024

time: 113 us -> 109 us (0.965)
  the two profiles are of different devices: /device:TPU:24 before, /device:TPU:95 now
where the time goes in v4:
time: 109 us
  Pallas kernels  107 us (98%)
  local copies, waits for them, and re-layouts  2.29 us (2%)
    pallas_call x1, Pallas kernels, per_device(): pl.pallas_call(kernel, out_shape=jax.ShapeDtypeStruct(gate.shape, bf), in...  107 us
    unnamed x1, local copies, waits for them, and re-layouts  2.29 us

profile of v4, /device:TPU:95, one launch (start us, length us, event | category | flops | bytes accessed | tf_op | source)
XLA Modules:
  0.0 109.2 jit_solution(17451860412026891499)
XLA Ops:
  0.0 106.9 %latent_attention.1 = bf16[128,4096]{1,0:T(8,128)(2,1)} custom-call(bf16[128,6144]{1,0:T(8,128)(2,1)} %q_ref.1, bf16[128,1024]{1,0:T(8,128)(2,1)} %lat_ref.1, bf16[64,128]{1,0:T(8,128)(2,1)} %bitcast.3, f32[1,1024]{1,0:T(1,128)} %bitcast.5, bf16[1024,1024]{1,0:T(8,128)(2,1)} %w_ref.1, bf16[128,4096]{1,0:T(8,128)(2,1)} %gate_ref.1, f32[1,4096]{1,0:T(1,128)} %bitcast.4, ...), custom_call_target="tpu_custom_call" | custom-call | tf_op jit(solution)/shard_map/latent_attention/pallas_call | solution.py:426
  106.9 2.3 %copy.12 = bf16[128,4096]{1,0:T(8,128)(2,1)} copy(bf16[128,4096]{1,0:T(8,128)(2,1)} %latent_attention.1) | data formatting | bytes 2097152
